TPU v7x, 256 devices: a whole 4x4x8 slice. The times are simulated.
256 devices in a mesh: sp: 64 (over z, x, core), tp: 4 (over y).
Axes of the slice: x: 4, y: 4, z: 8, core: 2. Of those that a mesh axis runs over, the one named last changes fastest.
Arguments:
- residual_in: bfloat16 [16384, 2048], P('sp', 'tp'), may hold values from -6 to 6
- conv_input: bfloat16 [16384, 512], P('sp', 'tp'), may hold values from -6 to 6
- outer_gate: bfloat16 [16384, 512], P('sp', 'tp'), may hold values from -6 to 6
- inner_gate: bfloat16 [16384, 512], P('sp', 'tp'), may hold values from -6 to 6
- documents: int32 [16384], P('sp'), may hold values from 0 to 31, as said below
- conv_taps: float32 [3, 512], P(None, 'tp'), may hold values from -3 to 3
- mixer_gain: float32 [512], replicated, may hold values from 0.1 to 1.9
- output_weight: bfloat16 [512, 2048], P(None, 'tp'), may hold values from -0.25 to 0.25
- ffn_gain: float32 [2048], P('tp'), may hold values from 0.1 to 1.9
- routes: int32 [16384, 2], P('sp'), may hold values from 0 to 63, all different within a row; in each aligned block of 256 rows (0 to 255, 256 to 511, ...) at most 16 rows name the same one
- route_weights: float32 [16384, 2], P('sp'), may hold values from 0.1 to 0.9
- expert_gate: bfloat16 [64, 2048, 3584], P('sp', None, 'tp'), may hold values from -0.125 to 0.125
- expert_up: bfloat16 [64, 2048, 3584], P('sp', None, 'tp'), may hold values from -0.125 to 0.125
- expert_down: bfloat16 [64, 3584, 2048], P('sp', 'tp'), may hold values from -0.09375 to 0.09375
Outputs:
- layer_out: bfloat16 [16384, 2048], P('sp', 'tp')
Inputs may be any that keep to these rules, and one draw needn't show every extreme that they name: Document numbers never fall along the positions, and each of the 32 documents occurs. Every document has 256 to 768 positions, and one has exactly 768. `routes`: the two experts of a position differ. Among the 256 positions of one index of sp no expert is named more than 16 times, a bound that some block reaches.
All inputs are finite; a program needn't handle non-finite values.
Results may differ from a plain program's by a relative error of at most 0.0058.
Values may be sent and summed in bfloat16 or wider, within the bound.
A program may use at most 64 MiB of HBM per device.

v0:
```python
import jax
import jax.numpy as jnp
from jax import lax
from jax.sharding import PartitionSpec as P

EPS = 1e-06


def from_behind(block, axis, distance):
    devices = range(lax.axis_size(axis))
    route = [(i - distance, i) for i in devices if i - distance in devices]
    return lax.ppermute(block, axis, route)


def laid_out(pieces, dim):
    dims = list(pieces.shape[1:])
    dims[dim] *= pieces.shape[0]
    return jnp.moveaxis(pieces, 0, dim).reshape(dims)


def sent_to_all(shard, axis):
    copies = jnp.broadcast_to(shard, (lax.axis_size(axis), *shard.shape))
    return lax.all_to_all(copies, axis, split_axis=0, concat_axis=0, tiled=True)


def gather_directly(shard, axis, dim):
    return laid_out(sent_to_all(shard, axis), dim)


def over_copies(shard, axis):
    return sent_to_all(shard, axis).sum(axis=0)


def slot_tables(routes, experts, capacity):
    tokens = routes.shape[0]
    flattened = routes.reshape(-1)
    onehot = (flattened[:, None] == jnp.arange(experts, dtype=jnp.int32)[None, :]).astype(jnp.int32)
    earlier = jnp.cumsum(onehot, axis=0) - onehot
    position_in = jnp.sum(earlier * onehot, axis=1)
    target = flattened * capacity + position_in
    owners = (
        jnp.full((experts * capacity,), tokens, jnp.int32)
        .at[target]
        .set(jnp.arange(2 * tokens, dtype=jnp.int32) // 2)
    )
    return (target, owners)


def per_device(
    residual_in,
    conv_input,
    outer_gate,
    inner_gate,
    documents,
    conv_taps,
    mixer_gain,
    output_weight,
    ffn_gain,
    routes,
    route_weights,
    expert_gate,
    expert_up,
    expert_down,
):
    tokens_here = residual_in.shape[0]
    local_features = residual_in.shape[1]
    conv_value = (inner_gate.astype(jnp.float32) * conv_input.astype(jnp.float32)).astype(
        jnp.bfloat16
    )
    doc_marks = documents.astype(jnp.bfloat16)
    before_rows, before_docs = from_behind((conv_value[-2:], doc_marks[-2:]), "sp", 1)
    joined_rows = jnp.concatenate([before_rows, conv_value], axis=0).astype(jnp.float32)
    joined_docs = jnp.concatenate([before_docs, doc_marks], axis=0)
    same_one = (joined_docs[1:-1] == doc_marks).astype(jnp.float32)[:, None]
    same_two = (joined_docs[:-2] == doc_marks).astype(jnp.float32)[:, None]
    conv_sum = (
        conv_taps[2] * joined_rows[2:]
        + conv_taps[1] * joined_rows[1:-1] * same_one
        + conv_taps[0] * joined_rows[:-2] * same_two
    )
    mixed = (outer_gate.astype(jnp.float32) * conv_sum).astype(jnp.bfloat16)
    piece_f = gather_directly(mixed, "tp", 1).astype(jnp.float32)
    scaled = (piece_f * mixer_gain).astype(jnp.bfloat16)
    accum = jnp.dot(scaled, output_weight, preferred_element_type=jnp.float32)
    squares = jnp.sum(piece_f * piece_f, axis=1)
    mix_scale = lax.rsqrt(squares / mixer_gain.shape[0] + EPS)
    hidden_state = residual_in.astype(jnp.float32) + accum * mix_scale[:, None]
    feature_total = over_copies(jnp.sum(hidden_state * hidden_state, axis=1), "tp")
    model_width = local_features * lax.axis_size("tp")
    normed = (
        hidden_state * lax.rsqrt(feature_total / model_width + EPS)[:, None] * ffn_gain
    ).astype(jnp.bfloat16)
    experts = lax.axis_size("sp") * expert_gate.shape[0]
    capacity = 4 * tokens_here // experts
    target, owners = slot_tables(routes, experts, capacity)
    padded = jnp.concatenate([normed, jnp.zeros((1, local_features), jnp.bfloat16)], axis=0)
    outgoing = padded[owners].reshape(experts, capacity, local_features)
    slices_in = lax.all_to_all(outgoing, "sp", split_axis=0, concat_axis=0, tiled=True)
    arrived = lax.all_gather(slices_in, "tp", axis=2, tiled=True)
    expert_in = arrived.reshape(-1, model_width)
    gate = jnp.dot(expert_in, expert_gate[0], preferred_element_type=jnp.float32)
    upper = jnp.dot(expert_in, expert_up[0], preferred_element_type=jnp.float32)
    act = (jax.nn.silu(gate) * upper).astype(jnp.bfloat16)
    partial_out = jnp.dot(act, expert_down[0], preferred_element_type=jnp.float32)
    summed = lax.psum_scatter(
        partial_out.astype(jnp.bfloat16), "tp", scatter_dimension=1, tiled=True
    )
    returned = lax.all_to_all(
        summed.reshape(experts, capacity, local_features),
        "sp",
        split_axis=0,
        concat_axis=0,
        tiled=True,
    )
    picked = returned.reshape(experts * capacity, local_features)[target].astype(jnp.float32)
    picked = picked.reshape(tokens_here, 2, local_features)
    routed = jnp.sum(picked * route_weights[:, :, None], axis=1)
    return (hidden_state + routed).astype(jnp.bfloat16)


def solution(mesh):
    placed = (
        P("sp", "tp"),
        P("sp", "tp"),
        P("sp", "tp"),
        P("sp", "tp"),
        P("sp"),
        P(None, "tp"),
        P(),
        P(None, "tp"),
        P("tp"),
        P("sp", None),
        P("sp", None),
        P("sp", None, "tp"),
        P("sp", None, "tp"),
        P("sp", "tp", None),
    )
    return jax.shard_map(
        per_device, mesh=mesh, in_specs=placed, out_specs=P("sp", "tp"), check_vma=False
    )
```

profile of v0, /device:TPU:1, one launch (start us, length us, event | category | flops | bytes accessed | tf_op | source)
XLA Modules:
  0.0 252.4 jit_solution(10328017283454354348)
XLA Ops:
  6.5 0.8 convert_element_type.78
  7.4 4.5 %collective-permute-start.1 = (bf16[2]{0:T(256)(128)(2,1)S(1)}, bf16[2]{0:T(256)(128)(2,1)S(1)}, u32[]{:S(2)}, u32[]{:S(2)}) collective-permute-start(bf16[2]{0:T(256)(128)(2,1)S(1)} %slice.41), channel_id=1, source_target_pairs={{0,4},{4,8},{8,12},{12,16},{16,20},{20,24},{24,28},{28,32},{32,36}... | collective-permute-start | bytes 20 | tf_op jit(solution)/shard_map/ppermute | solution.py:12
  11.9 0.9 multiply_convert_fusion.2
  12.8 1.9 collective-permute-start
  14.7 0.8 copy.31
  15.8 0.7 broadcast_multiply_fusion
  16.5 0.8 slice_bitcast_fusion.2
  17.3 1.2 reduce-window.6
  19.3 0.8 compare_convert_fusion.1
  20.1 1.0 fusion.15
  21.2 0.7 broadcast_in_dim.8
  21.9 4.2 %all-to-all-start = ((bf16[4,256,128]{1,2,0:T(8,128)(2,1)}), bf16[4,256,128]{1,2,0:T(8,128)(2,1)S(1)}, u32[]{:S(2)}, u32[]{:S(2)}) async-start(bf16[4,256,128]{1,2,0:T(8,128)(2,1)} %broadcast_in_dim.8), calls=%async_computation | async-start | bytes 524288 | tf_op jit(solution)/shard_map/all_to_all | solution.py:23
  26.1 2.4 scatter_custom_fusion
  28.5 3.2 %all-to-all-done = bf16[4,256,128]{1,2,0:T(8,128)(2,1)S(1)} async-done(((bf16[4,256,128]{1,2,0:T(8,128)(2,1)}), bf16[4,256,128]{1,2,0:T(8,128)(2,1)S(1)}, u32[]{:S(2)}, u32[]{:S(2)}) %all-to-all-start) | async-done | bytes 262176 | tf_op jit(solution)/shard_map/all_to_all | solution.py:23
  31.9 0.8 fusion.8
  32.7 0.4 multiply_reduce_fusion.1
  33.2 0.6 broadcast_in_dim.9
  33.8 3.2 %all-to-all-start.1 = ((f32[4,1,256]{2,1,0:T(1,128)}), f32[4,1,256]{2,1,0:T(1,128)S(1)}, u32[]{:S(2)}, u32[]{:S(2)}) async-start(f32[4,1,256]{2,1,0:T(1,128)} %broadcast_in_dim.9), calls=%async_computation.1 | async-start | bytes 8192 | tf_op jit(solution)/shard_map/all_to_all | solution.py:23
  37.1 4.0 %all-to-all-done.1 = f32[4,1,256]{2,1,0:T(1,128)S(1)} async-done(((f32[4,1,256]{2,1,0:T(1,128)}), f32[4,1,256]{2,1,0:T(1,128)S(1)}, u32[]{:S(2)}, u32[]{:S(2)}) %all-to-all-start.1) | async-done | bytes 4128 | tf_op jit(solution)/shard_map/all_to_all | solution.py:23
  41.3 4.0 %gather_fusion = bf16[1024,512]{1,0:T(8,128)(2,1)S(1)} fusion(bf16[257,512]{1,0:T(8,128)(2,1)S(1)} %concatenate.11, s32[1024]{0:T(1024)S(1)} %fusion.19), kind=kCustom, calls=%fused_computation | custom fusion | bytes 2101248 | tf_op jit(solution)/shard_map/gather | solution.py:97
  45.3 42.3 %all_to_all.21 = bf16[64,16,512]{2,1,0:T(8,128)(2,1)} all-to-all(bf16[64,16,512]{2,1,0:T(8,128)(2,1)S(1)} %bitcast.54), channel_id=1, replica_groups=mesh['sp'=64,'tp'=4] {'sp'}, dimensions={0} | all-to-all | bytes 2097152 | tf_op jit(solution)/shard_map/all_to_all | solution.py:98
  87.7 45.8 %all-gather.2.cloned.1.call-done = bf16[64,16,2048]{2,1,0:T(8,128)(2,1)} async-done(((bf16[64,16,512]{2,1,0:T(8,128)(2,1)}), bf16[64,16,2048]{2,1,0:T(8,128)(2,1)}) %all-gather.2.cloned.1.call-update) | async-done | bytes 4194320 | tf_op jit(solution)/shard_map/all_gather | solution.py:99
  133.5 7.5 %fusion.1 = f32[1024,896]{1,0:T(8,128)S(1)} fusion(bf16[1024,2048]{1,0:T(8,128)(2,1)} %bitcast.59, bf16[1,2048,896]{2,1,0:T(8,128)(2,1)} %param.26), kind=kOutput, calls=%fused_computation.5 | convolution fusion | flops 3758096384 | bytes 11534336 | tf_op jit(solution)/shard_map/dot_general | solution.py:102
  141.0 4.8 %multiply_convert_fusion = bf16[1024,896]{1,0:T(8,128)(2,1)S(1)} fusion(f32[1024,896]{1,0:T(8,128)S(1)} %fusion.1, bf16[1024,2048]{1,0:T(8,128)(2,1)S(1)} %bitcast.60, bf16[1,2048,896]{2,1,0:T(8,128)(2,1)S(1)} %copy-done.5), kind=kOutput, calls=%fused_computation.9 | convolution fusion | flops 3763601408 | bytes 13369344 | tf_op jit(solution)/shard_map/dot_general | solution.py:101
  145.9 6.1 %convolution_convert_fusion = bf16[1024,2048]{1,0:T(8,128)(2,1)} fusion(bf16[1024,896]{1,0:T(8,128)(2,1)S(1)} %multiply_convert_fusion, bf16[1,896,2048]{2,1,0:T(8,128)(2,1)S(1)} %copy-done.6), kind=kOutput, calls=%fused_computation.3 | convolution fusion | flops 3760193536 | bytes 9699328 | tf_op jit(solution)/shard_map/dot_general | solution.py:104
  151.9 50.0 %reduce-scatter.2.cloned.1.call-done = bf16[1024,512]{1,0:T(8,128)(2,1)} async-done(((bf16[1024,2048]{1,0:T(8,128)(2,1)}), bf16[1024,512]{1,0:T(8,128)(2,1)}) %reduce-scatter.2.cloned.1.call-update) | async-done | bytes 1048592 | tf_op jit(solution)/shard_map/reduce_scatter | solution.py:105
  202.0 10.7 %all-to-all-start.3 = ((bf16[64,16,512]{2,1,0:T(8,128)(2,1)}), bf16[64,16,512]{2,1,0:T(8,128)(2,1)S(1)}, u32[]{:S(2)}, u32[]{:S(2)}) async-start(bf16[64,16,512]{2,1,0:T(8,128)(2,1)} %bitcast.55), calls=%async_computation.4 | async-start | bytes 2097152 | tf_op jit(solution)/shard_map/all_to_all | solution.py:108
  212.8 28.0 %all-to-all-done.3 = bf16[64,16,512]{2,1,0:T(8,128)(2,1)S(1)} async-done(((bf16[64,16,512]{2,1,0:T(8,128)(2,1)}), bf16[64,16,512]{2,1,0:T(8,128)(2,1)S(1)}, u32[]{:S(2)}, u32[]{:S(2)}) %all-to-all-start.3) | async-done | bytes 1048608 | tf_op jit(solution)/shard_map/all_to_all | solution.py:108
  240.8 2.0 gather_fusion.1
  242.8 0.7 reshape.90
  243.5 1.3 multiply_reduce_fusion
  244.8 0.8 add_convert_fusion
  (45 shorter events, 1.8 us)
Async XLA Ops:
  6.5 26.2 %copy-start = (bf16[512,512]{1,0:T(8,128)(2,1)S(1)}, bf16[512,512]{1,0:T(8,128)(2,1)}, u32[]{:S(2)}) copy-start(bf16[512,512]{1,0:T(8,128)(2,1)} %param.21) | copy-start | bytes 1572868
  6.5 26.2 %copy-start.1 = (bf16[256,512]{1,0:T(8,128)(2,1)S(1)}, bf16[256,512]{1,0:T(8,128)(2,1)}, u32[]{:S(2)}) copy-start(bf16[256,512]{1,0:T(8,128)(2,1)} %param.14) | copy-start | bytes 786436
  6.5 34.6 %copy-start.2 = (f32[512]{0:T(512)S(1)}, f32[512]{0:T(512)}, u32[]{:S(2)}) copy-start(f32[512]{0:T(512)} %param.22) | copy-start | bytes 6148
  7.4 11.8 %collective-permute-start.1 = (bf16[2]{0:T(256)(128)(2,1)S(1)}, bf16[2]{0:T(256)(128)(2,1)S(1)}, u32[]{:S(2)}, u32[]{:S(2)}) collective-permute-start(bf16[2]{0:T(256)(128)(2,1)S(1)} %slice.41), channel_id=1, source_target_pairs={{0,4},{4,8},{8,12},{12,16},{16,20},{20,24},{24,28},{28,32},{32,36}... | collective-permute-start | bytes 20 | tf_op jit(solution)/shard_map/ppermute | solution.py:12
  12.8 7.3 %collective-permute-start = (bf16[2,128]{1,0:T(2,128)(2,1)S(1)}, bf16[2,128]{1,0:T(2,128)(2,1)S(1)}, u32[]{:S(2)}, u32[]{:S(2)}) collective-permute-start(bf16[2,128]{1,0:T(2,128)(2,1)S(1)} %slice.52), channel_id=1, source_target_pairs={{0,4},{4,8},{8,12},{12,16},{16,20},{20,24},{24,28},{28,32},{32,36}... | collective-permute-start | bytes 1544 | tf_op jit(solution)/shard_map/ppermute | solution.py:12
  21.9 9.9 %all-to-all-start = ((bf16[4,256,128]{1,2,0:T(8,128)(2,1)}), bf16[4,256,128]{1,2,0:T(8,128)(2,1)S(1)}, u32[]{:S(2)}, u32[]{:S(2)}) async-start(bf16[4,256,128]{1,2,0:T(8,128)(2,1)} %broadcast_in_dim.8), calls=%async_computation | async-start | bytes 524288 | tf_op jit(solution)/shard_map/all_to_all | solution.py:23
  33.8 7.4 %all-to-all-start.1 = ((f32[4,1,256]{2,1,0:T(1,128)}), f32[4,1,256]{2,1,0:T(1,128)S(1)}, u32[]{:S(2)}, u32[]{:S(2)}) async-start(f32[4,1,256]{2,1,0:T(1,128)} %broadcast_in_dim.9), calls=%async_computation.1 | async-start | bytes 8192 | tf_op jit(solution)/shard_map/all_to_all | solution.py:23
  37.0 96.5 %all-gather.2.cloned.1.call-start = ((), (), s32[]{:S(2)}) async-start(), calls=%async_computation.5 | async-start | bytes 5242880 | tf_op jit(solution)/shard_map/all_gather | solution.py:99
  87.7 114.3 %reduce-scatter.2.cloned.1.call-start = ((), (), s32[]{:S(2)}) async-start(), calls=%async_computation.6 | async-start | bytes 5242880 | tf_op jit(solution)/shard_map/reduce_scatter | solution.py:105
  133.5 7.5 %copy-start.4 = (bf16[64,16,2048]{2,1,0:T(8,128)(2,1)S(1)}, bf16[64,16,2048]{2,1,0:T(8,128)(2,1)}, u32[]{:S(2)}) copy-start(bf16[64,16,2048]{2,1,0:T(8,128)(2,1)} %all-gather.2.cloned.1.call-done) | copy-start | bytes 12582916
  133.5 7.5 %copy-start.5 = (bf16[1,2048,896]{2,1,0:T(8,128)(2,1)S(1)}, bf16[1,2048,896]{2,1,0:T(8,128)(2,1)}, u32[]{:S(2)}) copy-start(bf16[1,2048,896]{2,1,0:T(8,128)(2,1)} %param.25) | copy-start | bytes 11010052
  141.0 4.8 %copy-start.6 = (bf16[1,896,2048]{2,1,0:T(8,128)(2,1)S(1)}, bf16[1,896,2048]{2,1,0:T(8,128)(2,1)}, u32[]{:S(2)}) copy-start(bf16[1,896,2048]{2,1,0:T(8,128)(2,1)} %param.27) | copy-start | bytes 11010052
  151.9 60.8 %copy-start.3 = (f32[256,2]{0,1:T(2,128)S(1)}, f32[256,2]{0,1:T(2,128)}, u32[]{:S(2)}) copy-start(f32[256,2]{0,1:T(2,128)} %param.24) | copy-start | bytes 6148
  202.0 38.9 %all-to-all-start.3 = ((bf16[64,16,512]{2,1,0:T(8,128)(2,1)}), bf16[64,16,512]{2,1,0:T(8,128)(2,1)S(1)}, u32[]{:S(2)}, u32[]{:S(2)}) async-start(bf16[64,16,512]{2,1,0:T(8,128)(2,1)} %bitcast.55), calls=%async_computation.4 | async-start | bytes 2097152 | tf_op jit(solution)/shard_map/all_to_all | solution.py:108
Sparse Core Ops, SparseCore 0:
  87.8 45.6 all-gather.1
  152.1 49.8 reduce-scatter.1
where the time goes:
time: 253 us; the launch traced here: 252 us
  waiting for transfers between devices  131 us (52%)
  blocking collectives  42.3 us (17%)
  starting transfers between devices  24.6 us (10%)
  matrix products  18.8 us (7%)
  between operations  13.7 us (5%)
  local copies, waits for them, and re-layouts  13.1 us (5%)
  other arithmetic  8.73 us (3%)
    reduce_scatter x1, waiting for transfers between devices, per_device(): lax.psum_scatter(partial_out.astype(jnp.bfloat16), 'tp', scatter_dimensio...  50 us
    all_gather x1, waiting for transfers between devices, per_device(): arrived = lax.all_gather(slices_in, 'tp', axis=2, tiled=True)  45.8 us
    all_to_all x1, blocking collectives, per_device(): lax.all_to_all(outgoing, 'sp', split_axis=0, concat_axis=0, tiled=True)  42.3 us
    all_to_all x1, waiting for transfers between devices, per_device(): lax.all_to_all(summed.reshape(experts, capacity, local_features), 'sp', s...  28 us
    all_to_all x1, starting transfers between devices, per_device(): lax.all_to_all(summed.reshape(experts, capacity, local_features), 'sp', s...  10.7 us
    dot_general x1, matrix products, per_device(): upper = jnp.dot(expert_in, expert_up[0], preferred_element_type=jnp.float32)  7.49 us
    all_to_all x2, starting transfers between devices, sent_to_all(): return lax.all_to_all(copies, axis, split_axis=0, concat_axis=0, tiled=True)  7.43 us
    all_to_all x2, waiting for transfers between devices, sent_to_all(): return lax.all_to_all(copies, axis, split_axis=0, concat_axis=0, tiled=True)  7.29 us
  transfers between devices with their start and end apart: 7, of which 5 were waited for; matrix products, arithmetic and copies ran while one was open for 3% of the time, Pallas kernels for 0%

commit v1 on v0

--- a/solution.py
+++ b/solution.py
@@ -96,7 +96,13 @@
     padded = jnp.concatenate([normed, jnp.zeros((1, local_features), jnp.bfloat16)], axis=0)
     outgoing = padded[owners].reshape(experts, capacity, local_features)
     slices_in = lax.all_to_all(outgoing, "sp", split_axis=0, concat_axis=0, tiled=True)
-    arrived = lax.all_gather(slices_in, "tp", axis=2, tiled=True)
+    count = lax.axis_size("tp")
+    block_2, tiles = (slices_in, [slices_in])
+    for _ in range(count - 1):
+        block_2 = lax.ppermute(block_2, "tp", [(i_2, (i_2 + 1) % count) for i_2 in range(count)])
+        tiles.insert(0, block_2)
+    line = jnp.concatenate(tiles, axis=2)
+    arrived = jnp.roll(line, (lax.axis_index("tp") + 1) * slices_in.shape[2], axis=2)
     expert_in = arrived.reshape(-1, model_width)
     gate = jnp.dot(expert_in, expert_gate[0], preferred_element_type=jnp.float32)
     upper = jnp.dot(expert_in, expert_up[0], preferred_element_type=jnp.float32)

time: 253 us -> 284 us (1.12)
  waiting for transfers between devices: 131 us -> 156 us
  local copies, waits for them, and re-layouts: 13.1 us -> 21.3 us
    ppermute x0 -> x3, waiting for transfers between devices: none -> 71.9 us  [per_device(): lax.ppermute(block_2, 'tp', [(i_2, (i_2 + 1) % count) for i_2 in range(co...]
    all_gather x1 -> x0, waiting for transfers between devices: 45.8 us -> none  [per_device(): arrived = lax.all_gather(slices_in, 'tp', axis=2, tiled=True)]
    unnamed x16 -> x21, local copies, waits for them, and re-layouts: 0.97 us -> 8.65 us
  transfers between devices with their start and end apart: 7 -> 9, of which waited for: 5 -> 7; matrix products, arithmetic and copies ran while one was open for 3% -> 3% of each run, Pallas kernels for 0% -> 0%
where the time goes in v1:
time: 284 us; the launch traced here: 283 us
  waiting for transfers between devices  156 us (55%)
  blocking collectives  42.2 us (15%)
  starting transfers between devices  24.9 us (9%)
  local copies, waits for them, and re-layouts  21.3 us (8%)
  matrix products  16.6 us (6%)
  between operations  13.7 us (5%)
  other arithmetic  8.71 us (3%)
    ppermute x3, waiting for transfers between devices, per_device(): lax.ppermute(block_2, 'tp', [(i_2, (i_2 + 1) % count) for i_2 in range(co...  71.9 us
    reduce_scatter x1, waiting for transfers between devices, per_device(): lax.psum_scatter(partial_out.astype(jnp.bfloat16), 'tp', scatter_dimensio...  48.8 us
    all_to_all x1, blocking collectives, per_device(): lax.all_to_all(outgoing, 'sp', split_axis=0, concat_axis=0, tiled=True)  42.2 us
    all_to_all x1, waiting for transfers between devices, per_device(): lax.all_to_all(summed.reshape(experts, capacity, local_features), 'sp', s...  28 us
    all_to_all x1, starting transfers between devices, per_device(): lax.all_to_all(summed.reshape(experts, capacity, local_features), 'sp', s...  10.7 us
    unnamed x21, local copies, waits for them, and re-layouts  8.65 us
    all_to_all x2, starting transfers between devices, sent_to_all(): return lax.all_to_all(copies, axis, split_axis=0, concat_axis=0, tiled=True)  7.43 us
    all_to_all x2, waiting for transfers between devices, sent_to_all(): return lax.all_to_all(copies, axis, split_axis=0, concat_axis=0, tiled=True)  7.29 us
  transfers between devices with their start and end apart: 9, of which 7 were waited for; matrix products, arithmetic and copies ran while one was open for 3% of the time, Pallas kernels for 0%

profile of v1, /device:TPU:1, one launch (start us, length us, event | category | flops | bytes accessed | tf_op | source)
XLA Modules:
  0.0 283.4 jit_solution(13396922570356189599)
XLA Ops:
  7.4 4.5 %collective-permute-start.1 = (bf16[2]{0:T(256)(128)(2,1)S(1)}, bf16[2]{0:T(256)(128)(2,1)S(1)}, u32[]{:S(2)}, u32[]{:S(2)}) collective-permute-start(bf16[2]{0:T(256)(128)(2,1)S(1)} %slice.41), channel_id=1, source_target_pairs={{0,4},{4,8},{8,12},{12,16},{16,20},{20,24},{24,28},{28,32},{32,36}... | collective-permute-start | bytes 20 | tf_op jit(solution)/shard_map/ppermute | solution.py:12
  11.9 0.9 multiply_convert_fusion.2
  12.8 1.9 collective-permute-start
  14.7 0.8 copy.31
  16.5 0.8 slice_bitcast_fusion.2
  17.3 1.2 reduce-window.6
  20.1 1.0 fusion.15
  21.9 4.2 %all-to-all-start = ((bf16[4,256,128]{1,2,0:T(8,128)(2,1)}), bf16[4,256,128]{1,2,0:T(8,128)(2,1)S(1)}, u32[]{:S(2)}, u32[]{:S(2)}) async-start(bf16[4,256,128]{1,2,0:T(8,128)(2,1)} %broadcast_in_dim.8), calls=%async_computation | async-start | bytes 524288 | tf_op jit(solution)/shard_map/all_to_all | solution.py:23
  26.1 2.4 scatter_custom_fusion
  28.5 3.2 %all-to-all-done = bf16[4,256,128]{1,2,0:T(8,128)(2,1)S(1)} async-done(((bf16[4,256,128]{1,2,0:T(8,128)(2,1)}), bf16[4,256,128]{1,2,0:T(8,128)(2,1)S(1)}, u32[]{:S(2)}, u32[]{:S(2)}) %all-to-all-start) | async-done | bytes 262176 | tf_op jit(solution)/shard_map/all_to_all | solution.py:23
  31.9 0.8 fusion.8
  32.7 1.4 multiply_reduce_fusion.1
  34.7 3.2 %all-to-all-start.1 = ((f32[4,1,256]{2,1,0:T(1,128)}), f32[4,1,256]{2,1,0:T(1,128)S(1)}, u32[]{:S(2)}, u32[]{:S(2)}) async-start(f32[4,1,256]{2,1,0:T(1,128)} %broadcast_in_dim.9), calls=%async_computation.1 | async-start | bytes 8192 | tf_op jit(solution)/shard_map/all_to_all | solution.py:23
  38.0 4.0 %all-to-all-done.1 = f32[4,1,256]{2,1,0:T(1,128)S(1)} async-done(((f32[4,1,256]{2,1,0:T(1,128)}), f32[4,1,256]{2,1,0:T(1,128)S(1)}, u32[]{:S(2)}, u32[]{:S(2)}) %all-to-all-start.1) | async-done | bytes 4128 | tf_op jit(solution)/shard_map/all_to_all | solution.py:23
  42.2 4.0 %gather_fusion = bf16[1024,512]{1,0:T(8,128)(2,1)S(1)} fusion(bf16[257,512]{1,0:T(8,128)(2,1)S(1)} %concatenate.17, s32[1024]{0:T(1024)S(1)} %fusion.19), kind=kCustom, calls=%fused_computation | custom fusion | bytes 2101248 | tf_op jit(solution)/shard_map/gather | solution.py:97
  46.2 42.2 %all_to_all.21 = bf16[64,16,512]{2,1,0:T(8,128)(2,1)S(1)} all-to-all(bf16[64,16,512]{2,1,0:T(8,128)(2,1)S(1)} %bitcast.54), channel_id=1, replica_groups=mesh['sp'=64,'tp'=4] {'sp'}, dimensions={0} | all-to-all | bytes 2097152 | tf_op jit(solution)/shard_map/all_to_all | solution.py:98
  88.7 24.5 %collective-permute-done.2 = bf16[64,16,512]{2,1,0:T(8,128)(2,1)S(1)} collective-permute-done((bf16[64,16,512]{2,1,0:T(8,128)(2,1)S(1)}, bf16[64,16,512]{2,1,0:T(8,128)(2,1)S(1)}, u32[]{:S(2)}, u32[]{:S(2)}) %collective-permute-start.2) | collective-permute-done | bytes 1048608 | tf_op jit(solution)/shard_map/ppermute | solution.py:102
  113.2 24.0 %collective-permute-done.3 = bf16[64,16,512]{2,1,0:T(8,128)(2,1)} collective-permute-done((bf16[64,16,512]{2,1,0:T(8,128)(2,1)S(1)}, bf16[64,16,512]{2,1,0:T(8,128)(2,1)}, u32[]{:S(2)}, u32[]{:S(2)}) %collective-permute-start.3) | collective-permute-done | bytes 1048608 | tf_op jit(solution)/shard_map/ppermute | solution.py:102
  137.3 23.4 %collective-permute-done.4 = bf16[64,16,512]{2,1,0:T(8,128)(2,1)} collective-permute-done((bf16[64,16,512]{2,1,0:T(8,128)(2,1)}, bf16[64,16,512]{2,1,0:T(8,128)(2,1)}, u32[]{:S(2)}, u32[]{:S(2)}) %collective-permute-start.4) | collective-permute-done | bytes 1048608 | tf_op jit(solution)/shard_map/ppermute | solution.py:102
  160.6 1.4 constant_dynamic-update-slice_fusion.7
  162.0 1.4 constant_dynamic-update-slice_fusion.6
  163.7 1.4 constant_dynamic-update-slice_fusion.3
  165.1 1.4 constant_dynamic-update-slice_fusion.2
  167.2 1.7 copy-done.3
  168.9 4.5 %fusion.3 = f32[1024,896]{1,0:T(8,128)S(1)} fusion(bf16[1024,2048]{1,0:T(8,128)(2,1)S(1)} %bitcast.55, bf16[1,2048,896]{2,1,0:T(8,128)(2,1)S(1)} %copy-done.3), kind=kOutput, calls=%fused_computation.7 | convolution fusion | flops 3758096384 | bytes 11534336 | tf_op jit(solution)/shard_map/dot_general | solution.py:107
  173.4 4.7 %multiply_convert_fusion = bf16[1024,896]{1,0:T(8,128)(2,1)S(1)} fusion(f32[1024,896]{1,0:T(8,128)S(1)} %fusion.3, bf16[1024,2048]{1,0:T(8,128)(2,1)S(1)} %bitcast.56, bf16[1,2048,896]{2,1,0:T(8,128)(2,1)S(1)} %copy-done.4), kind=kOutput, calls=%fused_computation.9 | convolution fusion | flops 3763601408 | bytes 13369344 | tf_op jit(solution)/shard_map/dot_general | solution.py:108
  178.1 6.1 %convolution_convert_fusion = bf16[1024,2048]{1,0:T(8,128)(2,1)} fusion(bf16[1024,896]{1,0:T(8,128)(2,1)S(1)} %multiply_convert_fusion, bf16[1,896,2048]{2,1,0:T(8,128)(2,1)S(1)} %copy-done.5), kind=kOutput, calls=%fused_computation.3 | convolution fusion | flops 3760193536 | bytes 9699328 | tf_op jit(solution)/shard_map/dot_general | solution.py:110
  184.2 48.8 %reduce-scatter.2.cloned.1.call-done = bf16[1024,512]{1,0:T(8,128)(2,1)} async-done(((bf16[1024,2048]{1,0:T(8,128)(2,1)}), bf16[1024,512]{1,0:T(8,128)(2,1)}) %reduce-scatter.2.cloned.1.call-update) | async-done | bytes 1048592 | tf_op jit(solution)/shard_map/reduce_scatter | solution.py:111
  232.9 10.7 %all-to-all-start.3 = ((bf16[64,16,512]{2,1,0:T(8,128)(2,1)}), bf16[64,16,512]{2,1,0:T(8,128)(2,1)S(1)}, u32[]{:S(2)}, u32[]{:S(2)}) async-start(bf16[64,16,512]{2,1,0:T(8,128)(2,1)} %bitcast.57), calls=%async_computation.4 | async-start | bytes 2097152 | tf_op jit(solution)/shard_map/all_to_all | solution.py:114
  243.8 28.0 %all-to-all-done.3 = bf16[64,16,512]{2,1,0:T(8,128)(2,1)S(1)} async-done(((bf16[64,16,512]{2,1,0:T(8,128)(2,1)}), bf16[64,16,512]{2,1,0:T(8,128)(2,1)S(1)}, u32[]{:S(2)}, u32[]{:S(2)}) %all-to-all-start.3) | async-done | bytes 1048608 | tf_op jit(solution)/shard_map/all_to_all | solution.py:114
  271.8 2.0 gather_fusion.1
  274.5 1.3 multiply_reduce_fusion
  (55 shorter events, 7.9 us)
Async XLA Ops:
  6.5 26.2 %copy-start = (bf16[512,512]{1,0:T(8,128)(2,1)S(1)}, bf16[512,512]{1,0:T(8,128)(2,1)}, u32[]{:S(2)}) copy-start(bf16[512,512]{1,0:T(8,128)(2,1)} %param.21) | copy-start | bytes 1572868
  6.5 35.6 %copy-start.1 = (f32[512]{0:T(512)S(1)}, f32[512]{0:T(512)}, u32[]{:S(2)}) copy-start(f32[512]{0:T(512)} %param.22) | copy-start | bytes 6148
  7.4 11.8 %collective-permute-start.1 = (bf16[2]{0:T(256)(128)(2,1)S(1)}, bf16[2]{0:T(256)(128)(2,1)S(1)}, u32[]{:S(2)}, u32[]{:S(2)}) collective-permute-start(bf16[2]{0:T(256)(128)(2,1)S(1)} %slice.41), channel_id=1, source_target_pairs={{0,4},{4,8},{8,12},{12,16},{16,20},{20,24},{24,28},{28,32},{32,36}... | collective-permute-start | bytes 20 | tf_op jit(solution)/shard_map/ppermute | solution.py:12
  12.8 7.3 %collective-permute-start = (bf16[2,128]{1,0:T(2,128)(2,1)S(1)}, bf16[2,128]{1,0:T(2,128)(2,1)S(1)}, u32[]{:S(2)}, u32[]{:S(2)}) collective-permute-start(bf16[2,128]{1,0:T(2,128)(2,1)S(1)} %slice.52), channel_id=1, source_target_pairs={{0,4},{4,8},{8,12},{12,16},{16,20},{20,24},{24,28},{28,32},{32,36}... | collective-permute-start | bytes 1544 | tf_op jit(solution)/shard_map/ppermute | solution.py:12
  21.9 9.9 %all-to-all-start = ((bf16[4,256,128]{1,2,0:T(8,128)(2,1)}), bf16[4,256,128]{1,2,0:T(8,128)(2,1)S(1)}, u32[]{:S(2)}, u32[]{:S(2)}) async-start(bf16[4,256,128]{1,2,0:T(8,128)(2,1)} %broadcast_in_dim.8), calls=%async_computation | async-start | bytes 524288 | tf_op jit(solution)/shard_map/all_to_all | solution.py:23
  34.7 7.4 %all-to-all-start.1 = ((f32[4,1,256]{2,1,0:T(1,128)}), f32[4,1,256]{2,1,0:T(1,128)S(1)}, u32[]{:S(2)}, u32[]{:S(2)}) async-start(f32[4,1,256]{2,1,0:T(1,128)} %broadcast_in_dim.9), calls=%async_computation.1 | async-start | bytes 8192 | tf_op jit(solution)/shard_map/all_to_all | solution.py:23
  37.9 195.0 %reduce-scatter.2.cloned.1.call-start = ((), (), s32[]{:S(2)}) async-start(), calls=%async_computation.5 | async-start | bytes 5242880 | tf_op jit(solution)/shard_map/reduce_scatter | solution.py:111
  88.4 24.8 %collective-permute-start.2 = (bf16[64,16,512]{2,1,0:T(8,128)(2,1)S(1)}, bf16[64,16,512]{2,1,0:T(8,128)(2,1)S(1)}, u32[]{:S(2)}, u32[]{:S(2)}) collective-permute-start(bf16[64,16,512]{2,1,0:T(8,128)(2,1)S(1)} %all_to_all.21), channel_id=1, source_target_pairs={{0,1},{1,2},{2,3},{3,0},{4,5},{5,6},{6,7},{7,4},{8,9},{9,10},{10,1... | collective-permute-start | bytes 3145736 | tf_op jit(solution)/shard_map/ppermute | solution.py:102
  113.2 24.0 %collective-permute-start.3 = (bf16[64,16,512]{2,1,0:T(8,128)(2,1)S(1)}, bf16[64,16,512]{2,1,0:T(8,128)(2,1)}, u32[]{:S(2)}, u32[]{:S(2)}) collective-permute-start(bf16[64,16,512]{2,1,0:T(8,128)(2,1)S(1)} %collective-permute-done.2), channel_id=1, source_target_pairs={{0,1},{1,2},{2,3},{3,0},{4,5},{5,6},{6,7},{7,4},{8,9},{9,10},{10,1... | collective-permute-start | bytes 3145736 | tf_op jit(solution)/shard_map/ppermute | solution.py:102
  137.2 23.4 %collective-permute-start.4 = (bf16[64,16,512]{2,1,0:T(8,128)(2,1)}, bf16[64,16,512]{2,1,0:T(8,128)(2,1)}, u32[]{:S(2)}, u32[]{:S(2)}) collective-permute-start(bf16[64,16,512]{2,1,0:T(8,128)(2,1)} %collective-permute-done.3), channel_id=1, source_target_pairs={{0,1},{1,2},{2,3},{3,0},{4,5},{5,6},{6,7},{7,4},{8,9},{9,10},{10,1... | collective-permute-start | bytes 3145736 | tf_op jit(solution)/shard_map/ppermute | solution.py:102
  166.8 2.0 copy-start.3
  168.9 4.5 %copy-start.4 = (bf16[1,2048,896]{2,1,0:T(8,128)(2,1)S(1)}, bf16[1,2048,896]{2,1,0:T(8,128)(2,1)}, u32[]{:S(2)}) copy-start(bf16[1,2048,896]{2,1,0:T(8,128)(2,1)} %param.26) | copy-start | bytes 11010052
  173.4 4.7 %copy-start.5 = (bf16[1,896,2048]{2,1,0:T(8,128)(2,1)S(1)}, bf16[1,896,2048]{2,1,0:T(8,128)(2,1)}, u32[]{:S(2)}) copy-start(bf16[1,896,2048]{2,1,0:T(8,128)(2,1)} %param.27) | copy-start | bytes 11010052
  184.1 59.5 %copy-start.2 = (f32[256,2]{0,1:T(2,128)S(1)}, f32[256,2]{0,1:T(2,128)}, u32[]{:S(2)}) copy-start(f32[256,2]{0,1:T(2,128)} %param.24) | copy-start | bytes 6148
  232.9 38.9 %all-to-all-start.3 = ((bf16[64,16,512]{2,1,0:T(8,128)(2,1)}), bf16[64,16,512]{2,1,0:T(8,128)(2,1)S(1)}, u32[]{:S(2)}, u32[]{:S(2)}) async-start(bf16[64,16,512]{2,1,0:T(8,128)(2,1)} %bitcast.57), calls=%async_computation.4 | async-start | bytes 2097152 | tf_op jit(solution)/shard_map/all_to_all | solution.py:114
Sparse Core Ops, SparseCore 0:
  184.3 48.5 reduce-scatter.1
